TPU v7x, 256 devices: a whole 4x4x8 slice. The times are simulated.
256 devices in a mesh: ep: 32 (over z, x), tp: 8 (over y, core).
Axes of the slice: x: 4, y: 4, z: 8, core: 2. Of those that a mesh axis runs over, the one named last changes fastest.
Arguments:
- hidden: bfloat16 [1024, 4096], P('ep', 'tp'), may hold values from -6 to 6
- norm_gain: float32 [4096], P('tp'), may hold values from 0.1 to 1.9
- expert_ids: int32 [1024, 8], P('ep'), may hold values from 0 to 63, as said below
- route_weights: float32 [1024, 8], P('ep'), may hold values from 0.1 to 1
- lengths: int32 [128], P('ep'), may hold values from 1 to 8, as said below
- gate_proj: bfloat16 [64, 4096, 1024], P('ep', None, 'tp'), may hold values from -0.09375 to 0.09375
- up_proj: bfloat16 [64, 4096, 1024], P('ep', None, 'tp'), may hold values from -0.09375 to 0.09375
- down_proj: bfloat16 [64, 1024, 4096], P('ep', 'tp'), may hold values from -0.1875 to 0.1875
- shared_gate: bfloat16 [4096, 1024], P(None, 'tp'), may hold values from -0.09375 to 0.09375
- shared_up: bfloat16 [4096, 1024], P(None, 'tp'), may hold values from -0.09375 to 0.09375
- shared_down: bfloat16 [1024, 4096], P('tp'), may hold values from -0.1875 to 0.1875
Outputs:
- mixed: bfloat16 [1024, 4096], P('ep', 'tp')
Inputs may be any that keep to these rules, and one draw needn't show every extreme that they name: `expert_ids`: among the 32 rows of one index of ep (an aligned block), no expert is named more than 12 times, and in every block one expert is named exactly 12 times; each row names 8 different experts. `lengths`: each sequence has 1 to 8 live slots; on some index of ep all 4 sequences have 8 live slots.
All inputs are finite; a program needn't handle non-finite values.
Results may differ from a plain program's by a relative error of at most 0.015.
Values may be sent and summed in bfloat16 or wider, within the bound.
A program may use at most 128 MiB of HBM per device.

v0:
```python
import jax
import jax.numpy as jnp
from jax import lax
from jax.sharding import PartitionSpec as P

epsilon = 1e-06


def in_order(tiles, dim):
    lengths = list(tiles.shape[1:])
    lengths[dim] *= tiles.shape[0]
    return jnp.moveaxis(tiles, 0, dim).reshape(lengths)


def sent_to_all(value, axis):
    size = lax.axis_size(axis)
    return lax.all_to_all(
        jnp.broadcast_to(value[None], (size, *value.shape)), axis, 0, 0, tiled=True
    )


def gathered_copies(value, axis, dim):
    return in_order(sent_to_all(value, axis), dim)


def over_copies(value, axis):
    everything = sent_to_all(value, axis)
    return jnp.sum(everything, axis=0)


def cut_along(value, dim, size):
    before, after = (value.shape[:dim], value.shape[dim + 1 :])
    return jnp.moveaxis(value.reshape(*before, size, -1, *after), dim, 0)


def summed_on_arrival(value, axis, dim):
    tiles = cut_along(value, dim, lax.axis_size(axis))
    arrived = lax.all_to_all(tiles, axis, split_axis=0, concat_axis=0, tiled=True)
    return arrived.astype(jnp.float32).sum(axis=0)


def expert_inner(arrived, gate_proj, up_proj):
    gate_value = jnp.einsum(
        "gecd,edf->gecf", arrived, gate_proj, preferred_element_type=jnp.float32
    )
    up_value = jnp.einsum("gecd,edf->gecf", arrived, up_proj, preferred_element_type=jnp.float32)
    return (jax.nn.silu(gate_value) * up_value).astype(jnp.bfloat16)


def widen_rows(arrived):
    flat_rows = arrived.reshape(-1, arrived.shape[-1])
    widened = gathered_copies(flat_rows, "tp", 1)
    return widened.reshape(arrived.shape[:-1] + (widened.shape[1],))


def dispatch_plan(source_rows, expert_ids, is_live, expert_count, capacity, local_experts):
    slot_count, top_count = expert_ids.shape
    flat_ids = expert_ids.reshape(-1)
    flat_live = jnp.repeat(is_live, top_count)
    hit_matrix = (
        (flat_ids[:, None] == jnp.arange(expert_count, dtype=jnp.int32)[None, :])
        & flat_live[:, None]
    ).astype(jnp.int32)
    earlier = jnp.cumsum(hit_matrix, axis=0) - hit_matrix
    position = jnp.sum(hit_matrix * earlier, axis=1)
    total_slots = expert_count * capacity
    slot_index = jnp.where(flat_live, flat_ids * capacity + position, total_slots)
    chooser = jnp.any(
        slot_index.reshape(slot_count, top_count)[None, :, :]
        == jnp.arange(total_slots, dtype=jnp.int32)[:, None, None],
        axis=2,
    )
    outgoing = jnp.dot(
        chooser.astype(jnp.bfloat16), source_rows, preferred_element_type=jnp.float32
    ).astype(jnp.bfloat16)
    outgoing = outgoing.reshape(lax.axis_size("ep"), local_experts, capacity, source_rows.shape[1])
    return (outgoing, slot_index)


def collect_rows(returned, slot_index, mixing):
    slot_count, top_count = mixing.shape
    back_flat = returned.reshape(-1, returned.shape[3])
    total_slots = back_flat.shape[0]
    picked = jnp.take(back_flat, jnp.minimum(slot_index, total_slots - 1), axis=0)
    picked = picked.reshape(slot_count, top_count, back_flat.shape[1])
    return jnp.sum(mixing[:, :, None] * picked, axis=1)


def body(
    hidden,
    norm_gain,
    expert_ids,
    route_weights,
    lengths,
    gate_proj,
    up_proj,
    down_proj,
    shared_gate,
    shared_up,
    shared_down,
):
    slot_count = hidden.shape[0]
    top_count = expert_ids.shape[1]
    span_size = slot_count // lengths.shape[0]
    local_experts = gate_proj.shape[0]
    expert_count = local_experts * lax.axis_size("ep")
    capacity = min(
        slot_count, max(2, (3 * slot_count * top_count + expert_count - 1) // expert_count)
    )
    model_width = hidden.shape[1] * lax.axis_size("tp")
    values = hidden.astype(jnp.float32)
    squares = over_copies(jnp.sum(values * values, axis=1), "tp")
    row_scale = lax.rsqrt(squares / model_width + epsilon)
    normed = (values * row_scale[:, None] * norm_gain[None, :]).astype(jnp.bfloat16)
    full_rows = gathered_copies(normed, "tp", 1)
    offsets = jnp.arange(slot_count, dtype=jnp.int32) % span_size
    is_live = offsets < jnp.repeat(lengths, span_size)
    mixing = jnp.where(is_live[:, None], route_weights, 0.0)
    shared_inner = (
        jax.nn.silu(jnp.dot(full_rows, shared_gate, preferred_element_type=jnp.float32))
        * jnp.dot(full_rows, shared_up, preferred_element_type=jnp.float32)
    ).astype(jnp.bfloat16)
    shared_part = jnp.dot(shared_inner, shared_down, preferred_element_type=jnp.float32)
    outgoing, slot_index = dispatch_plan(
        normed, expert_ids, is_live, expert_count, capacity, local_experts
    )
    down_share = lax.all_to_all(down_proj, "tp", split_axis=2, concat_axis=1, tiled=True)
    inner_value = expert_inner(
        widen_rows(lax.all_to_all(outgoing, "ep", split_axis=0, concat_axis=0, tiled=True)),
        gate_proj,
        up_proj,
    )
    inner_whole = gathered_copies(inner_value, "tp", 3)
    result = jnp.einsum(
        "gecf,efd->gecd", inner_whole, down_share, preferred_element_type=jnp.float32
    )
    returned = lax.all_to_all(
        result.astype(jnp.bfloat16), "ep", split_axis=0, concat_axis=0, tiled=True
    ).astype(result.dtype)
    routed = collect_rows(returned, slot_index, mixing)
    combined = routed + summed_on_arrival(shared_part.astype(jnp.bfloat16), "tp", 1)
    return jnp.where(is_live[:, None], combined, 0.0).astype(jnp.bfloat16)


def solution(mesh):
    placed = (
        P("ep", "tp"),
        P("tp"),
        P("ep", None),
        P("ep", None),
        P("ep"),
        P("ep", None, "tp"),
        P("ep", None, "tp"),
        P("ep", "tp", None),
        P(None, "tp"),
        P(None, "tp"),
        P("tp", None),
    )
    return jax.shard_map(body, mesh=mesh, in_specs=placed, out_specs=P("ep", "tp"), check_vma=False)
```

profile of v0, /device:TPU:2, one launch (start us, length us, event | category | flops | bytes accessed | tf_op | source)
XLA Modules:
  0.0 256.2 jit_solution(8316562800688118385)
XLA Ops:
  0.0 1.0 fusion.39
  1.0 0.6 broadcast_in_dim.97
  1.6 4.5 %all-to-all-start = ((f32[8,1,32]{2,1,0:T(1,128)}), f32[8,1,32]{2,1,0:T(1,128)S(1)}, u32[]{:S(2)}, u32[]{:S(2)}) async-start(f32[8,1,32]{2,1,0:T(1,128)} %broadcast_in_dim.97), calls=%async_computation | async-start | bytes 8192 | tf_op jit(solution)/shard_map/all_to_all | solution.py:17
  6.1 0.8 copy.94
  6.9 0.1 eq.41
  7.0 0.1 reshape.156
  7.0 0.7 broadcast_in_dim.90
  7.9 0.1 broadcast_in_dim.92
  8.0 0.1 broadcast_in_dim.93
  8.0 0.1 broadcast_in_dim.94
  8.2 0.6 reduce-window.6
  8.8 0.2 slice_reduce_fusion
  9.0 0.7 broadcast_in_dim.86
  9.7 0.1 reshape.155
  9.8 0.1 broadcast_in_dim.88
  9.9 0.1 reshape.157
  10.0 0.1 fusion.44
  10.1 0.1 reduce_sum.50
  10.2 0.1 compare_and_fusion
  10.3 0.3 fusion.36
  10.6 0.7 all-to-all-done
  11.3 0.8 fusion.41
  12.2 1.3 convolution_convert_fusion.1
  13.5 1.2 reshape.159
  14.7 0.8 copy.99
  15.6 33.9 %all_to_all.54 = bf16[32,2,12,512]{3,1,2,0:T(2,128)(2,1)} all-to-all(bf16[32,2,12,512]{3,1,2,0:T(2,128)(2,1)S(1)} %copy.99), channel_id=1, replica_groups=mesh['ep'=32,'tp'=8] {'ep'}, dimensions={0} | all-to-all | bytes 1572864 | tf_op jit(solution)/shard_map/all_to_all | solution.py:129
  49.5 0.7 broadcast_in_dim.103
  50.2 4.4 %all-to-all-start.6 = ((bf16[8,32,512]{2,1,0:T(8,128)(2,1)}), bf16[8,32,512]{2,1,0:T(8,128)(2,1)S(1)}, u32[]{:S(2)}, u32[]{:S(2)}) async-start(bf16[8,32,512]{2,1,0:T(8,128)(2,1)} %broadcast_in_dim.103), calls=%async_computation.6 | async-start | bytes 524288 | tf_op jit(solution)/shard_map/all_to_all | solution.py:17
  54.6 1.3 copy.100
  56.0 1.1 broadcast_in_dim.98
  57.0 5.1 %all-to-all-done.6 = bf16[8,32,512]{2,1,0:T(8,128)(2,1)S(1)} async-done(((bf16[8,32,512]{2,1,0:T(8,128)(2,1)}), bf16[8,32,512]{2,1,0:T(8,128)(2,1)S(1)}, u32[]{:S(2)}, u32[]{:S(2)}) %all-to-all-start.6) | async-done | bytes 262176 | tf_op jit(solution)/shard_map/all_to_all | solution.py:17
  62.1 4.4 %broadcast_in_dim.99 = bf16[8,768,512]{2,1,0:T(8,128)(2,1)} broadcast(bf16[768,512]{1,0:T(8,128)(2,1)} %broadcast_in_dim.98), dimensions={1,2} | broadcast | bytes 7077888 | tf_op jit(solution)/shard_map/broadcast_in_dim | solution.py:18
  66.6 4.7 %all-to-all-start.2 = ((bf16[8,768,512]{2,1,0:T(8,128)(2,1)}), bf16[8,768,512]{2,1,0:T(8,128)(2,1)}, u32[]{:S(2)}, u32[]{:S(2)}) async-start(bf16[8,768,512]{2,1,0:T(8,128)(2,1)} %broadcast_in_dim.99), calls=%async_computation.2 | async-start | bytes 12582912 | tf_op jit(solution)/shard_map/all_to_all | solution.py:17
  71.3 6.2 %copy.105 = bf16[2,128,4096]{1,0,2:T(2,128)(2,1)} copy(bf16[2,128,4096]{2,1,0:T(8,128)(2,1)} %param.18) | data formatting | bytes 4194304 | tf_op args[7]
  77.5 66.0 %all-to-all-done.2 = bf16[8,768,512]{2,1,0:T(8,128)(2,1)} async-done(((bf16[8,768,512]{2,1,0:T(8,128)(2,1)}), bf16[8,768,512]{2,1,0:T(8,128)(2,1)}, u32[]{:S(2)}, u32[]{:S(2)}) %all-to-all-start.2) | async-done | bytes 6291488 | tf_op jit(solution)/shard_map/all_to_all | solution.py:17
  143.4 4.4 %all-to-all-start.4 = ((bf16[2,128,4096]{1,0,2:T(2,128)(2,1)}), bf16[2,128,4096]{1,0,2:T(2,128)(2,1)}, u32[]{:S(2)}, u32[]{:S(2)}) async-start(bf16[2,128,4096]{1,0,2:T(2,128)(2,1)} %copy.105), calls=%async_computation.4 | async-start | bytes 4194304 | tf_op jit(solution)/shard_map/all_to_all | solution.py:127
  147.8 9.0 %copy.101 = bf16[768,8,512]{2,1,0:T(8,128)(2,1)} copy(bf16[768,8,512]{2,0,1:T(8,128)(2,1)} %bitcast.2) | data formatting | bytes 12582912 | tf_op jit(solution)/shard_map/transpose | solution.py:12
  156.8 12.0 %reshape_reshape.3 = bf16[32,2,12,4096]{3,2,1,0:T(8,128)(2,1)} reshape(bf16[768,8,512]{2,1,0:T(8,128)(2,1)} %copy.101) | data formatting | bytes 12582912 | tf_op jit(solution)/shard_map/reshape;reshape | solution.py:53
  168.9 7.9 %fusion.15 = f32[32,2,12,128]{3,0,2,1:T(8,128)S(1)} fusion(bf16[2,4096,128]{2,1,0:T(8,128)(2,1)S(1)} %copy-done, bf16[32,2,12,4096]{3,2,1,0:T(8,128)(2,1)} %reshape_reshape.3), kind=kOutput, calls=%fused_computation.14 | convolution fusion | flops 805306368 | bytes 8781824 | tf_op jit(solution)/shard_map/gecd,edf->gecf/dot_general | solution.py:43
  176.8 4.3 %fusion.30 = bf16[32,2,12,128]{3,0,2,1:T(8,128)(2,1)S(1)} fusion(bf16[2,4096,128]{2,1,0:T(8,128)(2,1)S(1)} %copy-done.5, bf16[32,2,12,4096]{3,2,1,0:T(8,128)(2,1)S(1)} %copy-done.1, f32[32,2,12,128]{3,0,2,1:T(8,128)S(1)} %fusion.15), kind=kOutput, calls=%fused_computation.17 | convolution fusion | flops 805896192 | bytes 8978432 | tf_op jit(solution)/shard_map/gecd,edf->gecf/dot_general | solution.py:46
  181.1 1.5 broadcast_in_dim.100
  182.6 4.8 %all-to-all-start.3 = ((bf16[8,32,2,12,128]{4,1,3,2,0:T(8,128)(2,1)}), bf16[8,32,2,12,128]{4,1,3,2,0:T(8,128)(2,1)}, u32[]{:S(2)}, u32[]{:S(2)}) async-start(bf16[8,32,2,12,128]{4,1,3,2,0:T(8,128)(2,1)} %broadcast_in_dim.100), calls=%async_computation.3 | async-start | bytes 3145728 | tf_op jit(solution)/shard_map/all_to_all | solution.py:17
  187.4 1.0 copy.118
  188.4 0.3 fusion.57
  188.7 2.1 convolution_convert_fusion
  190.8 0.7 copy.142
  191.5 6.1 %copy.106 = bf16[2,128,8,512]{3,1,2,0:T(8,128)(2,1)} copy(bf16[2,128,8,512]{1,0,3,2:T(2,128)(2,1)} %bitcast.10) | data formatting | bytes 4194304 | tf_op jit(solution)/shard_map/all_to_all | solution.py:127
  197.6 11.4 %all-to-all-done.3 = bf16[8,32,2,12,128]{4,1,3,2,0:T(8,128)(2,1)} async-done(((bf16[8,32,2,12,128]{4,1,3,2,0:T(8,128)(2,1)}), bf16[8,32,2,12,128]{4,1,3,2,0:T(8,128)(2,1)}, u32[]{:S(2)}, u32[]{:S(2)}) %all-to-all-start.3) | async-done | bytes 1572896 | tf_op jit(solution)/shard_map/all_to_all | solution.py:17
  209.1 3.4 %all-to-all-start.7 = ((bf16[8,32,512]{2,1,0:T(8,128)(2,1)}), bf16[8,32,512]{2,1,0:T(8,128)(2,1)S(1)}, u32[]{:S(2)}, u32[]{:S(2)}) async-start(bf16[8,32,512]{2,1,0:T(8,128)(2,1)} %bitcast.94), calls=%async_computation.7 | async-start | bytes 524288 | tf_op jit(solution)/shard_map/all_to_all | solution.py:38
  212.5 3.0 %fusion.12 = bf16[32,2,12,512]{3,0,2,1:T(8,128)(2,1)S(1)} fusion(bf16[2,1024,512,1]{2,1,3,0:T(8,128)(2,1)} %bitcast.97, bf16[8,32,2,12,128]{4,1,3,2,0:T(8,128)(2,1)} %all-to-all-done.3), kind=kOutput, calls=%fused_computation.13 | convolution fusion | flops 805699584 | bytes 4456448 | tf_op jit(solution)/shard_map/gecf,efd->gecd/dot_general | solution.py:134
  215.6 1.7 copy.107
  217.2 2.7 %all-to-all-done.7 = bf16[8,32,512]{2,1,0:T(8,128)(2,1)S(1)} async-done(((bf16[8,32,512]{2,1,0:T(8,128)(2,1)}), bf16[8,32,512]{2,1,0:T(8,128)(2,1)S(1)}, u32[]{:S(2)}, u32[]{:S(2)}) %all-to-all-start.7) | async-done | bytes 262176 | tf_op jit(solution)/shard_map/all_to_all | solution.py:38
  219.9 5.6 %all-to-all-start.5 = ((bf16[32,2,12,512]{3,1,2,0:T(2,128)(2,1)}), bf16[32,2,12,512]{3,1,2,0:T(2,128)(2,1)S(1)}, u32[]{:S(2)}, u32[]{:S(2)}) async-start(bf16[32,2,12,512]{3,1,2,0:T(2,128)(2,1)} %copy.107), calls=%async_computation.5 | async-start | bytes 1572864 | tf_op jit(solution)/shard_map/all_to_all | solution.py:137
  225.5 0.1 reshape.163
  225.6 0.1 mul.76
  225.7 0.1 copy.93
  225.8 0.1 broadcast_select_fusion
  225.9 21.7 %all-to-all-done.5 = bf16[32,2,12,512]{3,1,2,0:T(2,128)(2,1)S(1)} async-done(((bf16[32,2,12,512]{3,1,2,0:T(2,128)(2,1)}), bf16[32,2,12,512]{3,1,2,0:T(2,128)(2,1)S(1)}, u32[]{:S(2)}, u32[]{:S(2)}) %all-to-all-start.5) | async-done | bytes 786464 | tf_op jit(solution)/shard_map/all_to_all | solution.py:137
  247.6 0.3 copy_convert_fusion
  247.8 2.3 copy.109
  250.1 2.6 reshape.167
  252.7 2.6 %gather_fusion = f32[256,512]{1,0:T(8,128)S(1)} fusion(f32[768,512]{1,0:T(8,128)} %reshape.167, s32[1024]{0:T(1024)S(1)} %pad_clamp_fusion), kind=kCustom, calls=%fused_computation | custom fusion | bytes 1049600 | tf_op jit(solution)/shard_map/jit(_take)/gather | solution.py:84
  255.3 0.2 fusion.38
  255.5 0.7 select_convert_fusion
  (25 shorter events, 0.3 us)
Async XLA Ops:
  0.0 168.9 %copy-start = (bf16[2,4096,128]{2,1,0:T(8,128)(2,1)S(1)}, bf16[2,4096,128]{2,1,0:T(8,128)(2,1)}, u32[]{:S(2)}) copy-start(bf16[2,4096,128]{2,1,0:T(8,128)(2,1)} %param.16) | copy-start | bytes 6291460
  1.6 9.7 %all-to-all-start = ((f32[8,1,32]{2,1,0:T(1,128)}), f32[8,1,32]{2,1,0:T(1,128)S(1)}, u32[]{:S(2)}, u32[]{:S(2)}) async-start(f32[8,1,32]{2,1,0:T(1,128)} %broadcast_in_dim.97), calls=%async_computation | async-start | bytes 8192 | tf_op jit(solution)/shard_map/all_to_all | solution.py:17
  50.2 11.9 %all-to-all-start.6 = ((bf16[8,32,512]{2,1,0:T(8,128)(2,1)}), bf16[8,32,512]{2,1,0:T(8,128)(2,1)S(1)}, u32[]{:S(2)}, u32[]{:S(2)}) async-start(bf16[8,32,512]{2,1,0:T(8,128)(2,1)} %broadcast_in_dim.103), calls=%async_computation.6 | async-start | bytes 524288 | tf_op jit(solution)/shard_map/all_to_all | solution.py:17
  62.1 4.4 %copy-start.3 = (bf16[8,32,512]{2,1,0:T(8,128)(2,1)}, bf16[8,32,512]{2,1,0:T(8,128)(2,1)S(1)}, u32[]{:S(2)}) copy-start(bf16[8,32,512]{2,1,0:T(8,128)(2,1)S(1)} %all-to-all-done.6) | copy-start | bytes 786436
  66.6 76.9 %all-to-all-start.2 = ((bf16[8,768,512]{2,1,0:T(8,128)(2,1)}), bf16[8,768,512]{2,1,0:T(8,128)(2,1)}, u32[]{:S(2)}, u32[]{:S(2)}) async-start(bf16[8,768,512]{2,1,0:T(8,128)(2,1)} %broadcast_in_dim.99), calls=%async_computation.2 | async-start | bytes 12582912 | tf_op jit(solution)/shard_map/all_to_all | solution.py:17
  143.4 37.7 %all-to-all-start.4 = ((bf16[2,128,4096]{1,0,2:T(2,128)(2,1)}), bf16[2,128,4096]{1,0,2:T(2,128)(2,1)}, u32[]{:S(2)}, u32[]{:S(2)}) async-start(bf16[2,128,4096]{1,0,2:T(2,128)(2,1)} %copy.105), calls=%async_computation.4 | async-start | bytes 4194304 | tf_op jit(solution)/shard_map/all_to_all | solution.py:127
  168.9 7.9 %copy-start.1 = (bf16[32,2,12,4096]{3,2,1,0:T(8,128)(2,1)S(1)}, bf16[32,2,12,4096]{3,2,1,0:T(8,128)(2,1)}, u32[]{:S(2)}) copy-start(bf16[32,2,12,4096]{3,2,1,0:T(8,128)(2,1)} %reshape_reshape.3) | copy-start | bytes 18874372
  168.9 7.9 %copy-start.5 = (bf16[2,4096,128]{2,1,0:T(8,128)(2,1)S(1)}, bf16[2,4096,128]{2,1,0:T(8,128)(2,1)}, u32[]{:S(2)}) copy-start(bf16[2,4096,128]{2,1,0:T(8,128)(2,1)} %param.17) | copy-start | bytes 6291460
  182.6 5.8 %copy-start.2 = (bf16[4096,128]{1,0:T(8,128)(2,1)S(1)}, bf16[4096,128]{1,0:T(8,128)(2,1)}, u32[]{:S(2)}) copy-start(bf16[4096,128]{1,0:T(8,128)(2,1)} %param.19) | copy-start | bytes 3145732
  182.6 26.5 %all-to-all-start.3 = ((bf16[8,32,2,12,128]{4,1,3,2,0:T(8,128)(2,1)}), bf16[8,32,2,12,128]{4,1,3,2,0:T(8,128)(2,1)}, u32[]{:S(2)}, u32[]{:S(2)}) async-start(bf16[8,32,2,12,128]{4,1,3,2,0:T(8,128)(2,1)} %broadcast_in_dim.100), calls=%async_computation.3 | async-start | bytes 3145728 | tf_op jit(solution)/shard_map/all_to_all | solution.py:17
  209.1 10.8 %all-to-all-start.7 = ((bf16[8,32,512]{2,1,0:T(8,128)(2,1)}), bf16[8,32,512]{2,1,0:T(8,128)(2,1)S(1)}, u32[]{:S(2)}, u32[]{:S(2)}) async-start(bf16[8,32,512]{2,1,0:T(8,128)(2,1)} %bitcast.94), calls=%async_computation.7 | async-start | bytes 524288 | tf_op jit(solution)/shard_map/all_to_all | solution.py:38
  215.5 10.2 %copy-start.4 = (f32[32,8]{0,1:T(8,128)S(1)}, f32[32,8]{0,1:T(8,128)}, u32[]{:S(2)}) copy-start(f32[32,8]{0,1:T(8,128)} %param.14) | copy-start | bytes 3076
  219.9 27.7 %all-to-all-start.5 = ((bf16[32,2,12,512]{3,1,2,0:T(2,128)(2,1)}), bf16[32,2,12,512]{3,1,2,0:T(2,128)(2,1)S(1)}, u32[]{:S(2)}, u32[]{:S(2)}) async-start(bf16[32,2,12,512]{3,1,2,0:T(2,128)(2,1)} %copy.107), calls=%async_computation.5 | async-start | bytes 1572864 | tf_op jit(solution)/shard_map/all_to_all | solution.py:137
where the time goes:
time: 258 us; the launch traced here: 256 us
  waiting for transfers between devices  108 us (42%)
  local copies, waits for them, and re-layouts  59.4 us (23%)
  blocking collectives  33.9 us (13%)
  starting transfers between devices  31.8 us (12%)
  matrix products  18.9 us (7%)
  other arithmetic  4.39 us (2%)
    all_to_all x4, waiting for transfers between devices, sent_to_all(): lax.all_to_all(jnp.broadcast_to(value[None], (size, *value.shape)), axis,...  83.2 us
    all_to_all x1, blocking collectives, body(): lax.all_to_all(outgoing, 'ep', split_axis=0, concat_axis=0, tiled=True)  33.9 us
    all_to_all x1, waiting for transfers between devices, body(): lax.all_to_all(result.astype(jnp.bfloat16), 'ep', split_axis=0, concat_ax...  21.7 us
    all_to_all x4, starting transfers between devices, sent_to_all(): lax.all_to_all(jnp.broadcast_to(value[None], (size, *value.shape)), axis,...  18.4 us
    another operation x1, local copies, waits for them, and re-layouts, widen_rows(): return widened.reshape(arrived.shape[:-1] + (widened.shape[1],))  12 us
    transpose x1, local copies, waits for them, and re-layouts, in_order(): return jnp.moveaxis(tiles, 0, dim).reshape(lengths)  9.03 us
    broadcast_in_dim x5, local copies, waits for them, and re-layouts, sent_to_all(): jnp.broadcast_to(value[None], (size, *value.shape))  8.3 us
    dot_general x1, matrix products, expert_inner(): jnp.einsum('gecd,edf->gecf', arrived, gate_proj, preferred_element_type=j...  7.85 us
  transfers between devices with their start and end apart: 7, of which 6 were waited for; matrix products, arithmetic and copies ran while one was open for 24% of the time, Pallas kernels for 0%

commit v1 on v0

--- a/solution.py
+++ b/solution.py
@@ -124,7 +124,10 @@
     outgoing, slot_index = dispatch_plan(
         normed, expert_ids, is_live, expert_count, capacity, local_experts
     )
-    down_share = lax.all_to_all(down_proj, "tp", split_axis=2, concat_axis=1, tiled=True)
+    down_share = jnp.concatenate(
+        lax.all_to_all(jnp.stack(jnp.split(down_proj, lax.axis_size("tp"), axis=2)), "tp", 0, 0),
+        axis=1,
+    )
     inner_value = expert_inner(
         widen_rows(lax.all_to_all(outgoing, "ep", split_axis=0, concat_axis=0, tiled=True)),
         gate_proj,

time: 258 us -> 258 us (level)
  waiting for transfers between devices: 108 us -> 103 us
  local copies, waits for them, and re-layouts: 59.4 us -> 63.7 us
    all_to_all x1 -> x0, local copies, waits for them, and re-layouts: 6.14 us -> none  [body(): lax.all_to_all(down_proj, 'tp', split_axis=2, concat_axis=1, tiled=True)]
    unnamed x15 -> x21, local copies, waits for them, and re-layouts: 7.02 us -> 12.6 us
    all_to_all x4, waiting for transfers between devices: 83.2 us -> 79 us  [sent_to_all(): lax.all_to_all(jnp.broadcast_to(value[None], (size, *value.shape)), axis,...]
    reshape x0 -> x1, local copies, waits for them, and re-layouts: none -> 3.13 us  [body(): jnp.concatenate(lax.all_to_all(jnp.stack(jnp.split(down_proj, lax.axis_si...]
  transfers between devices with their start and end apart: 7 -> 7, of which waited for: 6 -> 6; matrix products, arithmetic and copies ran while one was open for 24% -> 26% of each run, Pallas kernels for 0% -> 0%
where the time goes in v1:
time: 258 us; the launch traced here: 256 us
  waiting for transfers between devices  103 us (40%)
  local copies, waits for them, and re-layouts  63.7 us (25%)
  blocking collectives  33.9 us (13%)
  starting transfers between devices  31.8 us (12%)
  matrix products  18.8 us (7%)
  other arithmetic  4.39 us (2%)
    all_to_all x4, waiting for transfers between devices, sent_to_all(): lax.all_to_all(jnp.broadcast_to(value[None], (size, *value.shape)), axis,...  79 us
    all_to_all x1, blocking collectives, body(): lax.all_to_all(outgoing, 'ep', split_axis=0, concat_axis=0, tiled=True)  33.9 us
    all_to_all x1, waiting for transfers between devices, body(): lax.all_to_all(result.astype(jnp.bfloat16), 'ep', split_axis=0, concat_ax...  21.7 us
    all_to_all x4, starting transfers between devices, sent_to_all(): lax.all_to_all(jnp.broadcast_to(value[None], (size, *value.shape)), axis,...  18.4 us
    unnamed x21, local copies, waits for them, and re-layouts  12.6 us
    another operation x1, local copies, waits for them, and re-layouts, widen_rows(): return widened.reshape(arrived.shape[:-1] + (widened.shape[1],))  12 us
    transpose x1, local copies, waits for them, and re-layouts, in_order(): return jnp.moveaxis(tiles, 0, dim).reshape(lengths)  9.03 us
    broadcast_in_dim x5, local copies, waits for them, and re-layouts, sent_to_all(): jnp.broadcast_to(value[None], (size, *value.shape))  8.3 us
  transfers between devices with their start and end apart: 7, of which 6 were waited for; matrix products, arithmetic and copies ran while one was open for 26% of the time, Pallas kernels for 0%

profile of v1, /device:TPU:2, one launch (start us, length us, event | category | flops | bytes accessed | tf_op | source)
XLA Modules:
  0.0 256.2 jit_solution(266614098668414876)
XLA Ops:
  0.0 1.0 fusion.39
  1.0 0.6 broadcast_in_dim.97
  1.6 4.5 %all-to-all-start.1 = ((f32[8,1,32]{2,1,0:T(1,128)}), f32[8,1,32]{2,1,0:T(1,128)S(1)}, u32[]{:S(2)}, u32[]{:S(2)}) async-start(f32[8,1,32]{2,1,0:T(1,128)} %broadcast_in_dim.97), calls=%async_computation.1 | async-start | bytes 8192 | tf_op jit(solution)/shard_map/all_to_all | solution.py:17
  6.1 0.8 copy.90
  6.9 0.1 eq.41
  7.0 0.1 reshape.162
  7.0 0.7 broadcast_in_dim.90
  8.0 0.1 broadcast_in_dim.94
  8.2 0.6 reduce-window.6
  8.8 0.2 slice_reduce_fusion
  9.0 0.7 broadcast_in_dim.86
  9.9 0.1 reshape.163
  10.0 0.1 fusion.44
  10.2 0.1 compare_and_fusion
  10.3 0.3 fusion.36
  10.6 0.7 all-to-all-done.1
  11.3 0.8 fusion.41
  12.2 1.3 convolution_convert_fusion.1
  13.5 1.2 reshape.167
  14.7 0.8 copy.96
  15.6 33.9 %all_to_all.41 = bf16[32,2,12,512]{3,1,2,0:T(2,128)(2,1)} all-to-all(bf16[32,2,12,512]{3,1,2,0:T(2,128)(2,1)S(1)} %copy.96), channel_id=1, replica_groups=mesh['ep'=32,'tp'=8] {'ep'}, dimensions={0} | all-to-all | bytes 1572864 | tf_op jit(solution)/shard_map/all_to_all | solution.py:132
  49.5 0.7 broadcast_in_dim.103
  50.2 4.4 %all-to-all-start.6 = ((bf16[8,32,512]{2,1,0:T(8,128)(2,1)}), bf16[8,32,512]{2,1,0:T(8,128)(2,1)S(1)}, u32[]{:S(2)}, u32[]{:S(2)}) async-start(bf16[8,32,512]{2,1,0:T(8,128)(2,1)} %broadcast_in_dim.103), calls=%async_computation.6 | async-start | bytes 524288 | tf_op jit(solution)/shard_map/all_to_all | solution.py:17
  54.6 1.3 copy.97
  56.0 1.1 broadcast_in_dim.98
  57.0 5.1 %all-to-all-done.6 = bf16[8,32,512]{2,1,0:T(8,128)(2,1)S(1)} async-done(((bf16[8,32,512]{2,1,0:T(8,128)(2,1)}), bf16[8,32,512]{2,1,0:T(8,128)(2,1)S(1)}, u32[]{:S(2)}, u32[]{:S(2)}) %all-to-all-start.6) | async-done | bytes 262176 | tf_op jit(solution)/shard_map/all_to_all | solution.py:17
  62.1 4.4 %broadcast_in_dim.99 = bf16[8,768,512]{2,1,0:T(8,128)(2,1)} broadcast(bf16[768,512]{1,0:T(8,128)(2,1)} %broadcast_in_dim.98), dimensions={1,2} | broadcast | bytes 7077888 | tf_op jit(solution)/shard_map/broadcast_in_dim | solution.py:18
  66.6 4.7 %all-to-all-start.3 = ((bf16[8,768,512]{2,1,0:T(8,128)(2,1)}), bf16[8,768,512]{2,1,0:T(8,128)(2,1)}, u32[]{:S(2)}, u32[]{:S(2)}) async-start(bf16[8,768,512]{2,1,0:T(8,128)(2,1)} %broadcast_in_dim.99), calls=%async_computation.3 | async-start | bytes 12582912 | tf_op jit(solution)/shard_map/all_to_all | solution.py:17
  71.3 1.7 bitcast_dynamic-update-slice_fusion.7
  73.0 1.7 bitcast_dynamic-update-slice_fusion.6
  74.6 1.7 bitcast_dynamic-update-slice_fusion.5
  76.3 1.7 bitcast_dynamic-update-slice_fusion.4
  78.0 1.7 bitcast_dynamic-update-slice_fusion.3
  79.7 1.7 bitcast_dynamic-update-slice_fusion.2
  81.4 1.7 bitcast_dynamic-update-slice_fusion.1
  83.1 1.7 bitcast_dynamic-update-slice_fusion
  84.7 58.7 %all-to-all-done.3 = bf16[8,768,512]{2,1,0:T(8,128)(2,1)} async-done(((bf16[8,768,512]{2,1,0:T(8,128)(2,1)}), bf16[8,768,512]{2,1,0:T(8,128)(2,1)}, u32[]{:S(2)}, u32[]{:S(2)}) %all-to-all-start.3) | async-done | bytes 6291488 | tf_op jit(solution)/shard_map/all_to_all | solution.py:17
  143.4 4.4 %all-to-all-start = ((bf16[8,2,128,512]{3,2,1,0:T(8,128)(2,1)}), bf16[8,2,128,512]{3,2,1,0:T(8,128)(2,1)}, u32[]{:S(2)}, u32[]{:S(2)}) async-start(bf16[8,2,128,512]{3,2,1,0:T(8,128)(2,1)} %bitcast_dynamic-update-slice_fusion), calls=%async_computation | async-start | bytes 4194304 | tf_op jit(solution)/shard_map/all_to_all | solution.py:128
  147.8 9.0 %copy.98 = bf16[768,8,512]{2,1,0:T(8,128)(2,1)} copy(bf16[768,8,512]{2,0,1:T(8,128)(2,1)} %bitcast.14) | data formatting | bytes 12582912 | tf_op jit(solution)/shard_map/transpose | solution.py:12
  156.8 12.0 %reshape_reshape.3 = bf16[32,2,12,4096]{3,2,1,0:T(8,128)(2,1)} reshape(bf16[768,8,512]{2,1,0:T(8,128)(2,1)} %copy.98) | data formatting | bytes 12582912 | tf_op jit(solution)/shard_map/reshape;reshape | solution.py:53
  168.9 7.9 %fusion.15 = f32[32,2,12,128]{3,0,2,1:T(8,128)S(1)} fusion(bf16[2,4096,128]{2,1,0:T(8,128)(2,1)S(1)} %copy-done, bf16[32,2,12,4096]{3,2,1,0:T(8,128)(2,1)} %reshape_reshape.3), kind=kOutput, calls=%fused_computation.14 | convolution fusion | flops 805306368 | bytes 8781824 | tf_op jit(solution)/shard_map/gecd,edf->gecf/dot_general | solution.py:43
  176.8 4.3 %fusion.30 = bf16[32,2,12,128]{3,0,2,1:T(8,128)(2,1)S(1)} fusion(bf16[2,4096,128]{2,1,0:T(8,128)(2,1)S(1)} %copy-done.5, bf16[32,2,12,4096]{3,2,1,0:T(8,128)(2,1)S(1)} %copy-done.1, f32[32,2,12,128]{3,0,2,1:T(8,128)S(1)} %fusion.15), kind=kOutput, calls=%fused_computation.17 | convolution fusion | flops 805896192 | bytes 8978432 | tf_op jit(solution)/shard_map/gecd,edf->gecf/dot_general | solution.py:46
  181.1 1.5 broadcast_in_dim.100
  182.6 4.8 %all-to-all-start.4 = ((bf16[8,32,2,12,128]{4,1,3,2,0:T(8,128)(2,1)}), bf16[8,32,2,12,128]{4,1,3,2,0:T(8,128)(2,1)}, u32[]{:S(2)}, u32[]{:S(2)}) async-start(bf16[8,32,2,12,128]{4,1,3,2,0:T(8,128)(2,1)} %broadcast_in_dim.100), calls=%async_computation.4 | async-start | bytes 3145728 | tf_op jit(solution)/shard_map/all_to_all | solution.py:17
  187.4 1.0 copy.113
  188.4 0.3 fusion.57
  188.7 2.1 convolution_convert_fusion
  190.8 0.7 copy.137
  191.5 3.1 %copy.94 = bf16[2,8,128,512]{3,2,1,0:T(8,128)(2,1)} copy(bf16[2,8,128,512]{3,2,0,1:T(8,128)(2,1)} %bitcast.9) | data formatting | bytes 4194304 | tf_op jit(solution)/shard_map/reshape | solution.py:127
  194.6 14.4 %all-to-all-done.4 = bf16[8,32,2,12,128]{4,1,3,2,0:T(8,128)(2,1)} async-done(((bf16[8,32,2,12,128]{4,1,3,2,0:T(8,128)(2,1)}), bf16[8,32,2,12,128]{4,1,3,2,0:T(8,128)(2,1)}, u32[]{:S(2)}, u32[]{:S(2)}) %all-to-all-start.4) | async-done | bytes 1572896 | tf_op jit(solution)/shard_map/all_to_all | solution.py:17
  209.1 3.4 %all-to-all-start.7 = ((bf16[8,32,512]{2,1,0:T(8,128)(2,1)}), bf16[8,32,512]{2,1,0:T(8,128)(2,1)S(1)}, u32[]{:S(2)}, u32[]{:S(2)}) async-start(bf16[8,32,512]{2,1,0:T(8,128)(2,1)} %bitcast.108), calls=%async_computation.7 | async-start | bytes 524288 | tf_op jit(solution)/shard_map/all_to_all | solution.py:38
  212.5 3.0 %fusion.12 = bf16[32,2,12,512]{3,0,2,1:T(8,128)(2,1)S(1)} fusion(bf16[2,1024,512,1]{2,1,3,0:T(8,128)(2,1)} %bitcast.111, bf16[8,32,2,12,128]{4,1,3,2,0:T(8,128)(2,1)} %all-to-all-done.4), kind=kOutput, calls=%fused_computation.13 | convolution fusion | flops 805699584 | bytes 4456448 | tf_op jit(solution)/shard_map/gecf,efd->gecd/dot_general | solution.py:137
  215.5 1.7 copy.102
  217.2 2.7 %all-to-all-done.7 = bf16[8,32,512]{2,1,0:T(8,128)(2,1)S(1)} async-done(((bf16[8,32,512]{2,1,0:T(8,128)(2,1)}), bf16[8,32,512]{2,1,0:T(8,128)(2,1)S(1)}, u32[]{:S(2)}, u32[]{:S(2)}) %all-to-all-start.7) | async-done | bytes 262176 | tf_op jit(solution)/shard_map/all_to_all | solution.py:38
  219.9 5.6 %all-to-all-start.5 = ((bf16[32,2,12,512]{3,1,2,0:T(2,128)(2,1)}), bf16[32,2,12,512]{3,1,2,0:T(2,128)(2,1)S(1)}, u32[]{:S(2)}, u32[]{:S(2)}) async-start(bf16[32,2,12,512]{3,1,2,0:T(2,128)(2,1)} %copy.102), calls=%async_computation.5 | async-start | bytes 1572864 | tf_op jit(solution)/shard_map/all_to_all | solution.py:140
  225.5 0.1 reshape.171
  225.6 0.1 mul.76
  225.9 21.7 %all-to-all-done.5 = bf16[32,2,12,512]{3,1,2,0:T(2,128)(2,1)S(1)} async-done(((bf16[32,2,12,512]{3,1,2,0:T(2,128)(2,1)}), bf16[32,2,12,512]{3,1,2,0:T(2,128)(2,1)S(1)}, u32[]{:S(2)}, u32[]{:S(2)}) %all-to-all-start.5) | async-done | bytes 786464 | tf_op jit(solution)/shard_map/all_to_all | solution.py:140
  247.6 0.3 copy_convert_fusion
  247.9 2.3 copy.104
  250.1 2.6 reshape.175
  252.7 2.6 %gather_fusion = f32[256,512]{1,0:T(8,128)S(1)} fusion(f32[768,512]{1,0:T(8,128)} %reshape.175, s32[1024]{0:T(1024)S(1)} %pad_clamp_fusion), kind=kCustom, calls=%fused_computation | custom fusion | bytes 1049600 | tf_op jit(solution)/shard_map/jit(_take)/gather | solution.py:84
  255.3 0.2 fusion.38
  255.5 0.7 select_convert_fusion
  (32 shorter events, 0.8 us)
Async XLA Ops:
  0.0 168.9 %copy-start = (bf16[2,4096,128]{2,1,0:T(8,128)(2,1)S(1)}, bf16[2,4096,128]{2,1,0:T(8,128)(2,1)}, u32[]{:S(2)}) copy-start(bf16[2,4096,128]{2,1,0:T(8,128)(2,1)} %param.16) | copy-start | bytes 6291460
  1.6 9.7 %all-to-all-start.1 = ((f32[8,1,32]{2,1,0:T(1,128)}), f32[8,1,32]{2,1,0:T(1,128)S(1)}, u32[]{:S(2)}, u32[]{:S(2)}) async-start(f32[8,1,32]{2,1,0:T(1,128)} %broadcast_in_dim.97), calls=%async_computation.1 | async-start | bytes 8192 | tf_op jit(solution)/shard_map/all_to_all | solution.py:17
  50.2 11.9 %all-to-all-start.6 = ((bf16[8,32,512]{2,1,0:T(8,128)(2,1)}), bf16[8,32,512]{2,1,0:T(8,128)(2,1)S(1)}, u32[]{:S(2)}, u32[]{:S(2)}) async-start(bf16[8,32,512]{2,1,0:T(8,128)(2,1)} %broadcast_in_dim.103), calls=%async_computation.6 | async-start | bytes 524288 | tf_op jit(solution)/shard_map/all_to_all | solution.py:17
  62.1 4.4 %copy-start.3 = (bf16[8,32,512]{2,1,0:T(8,128)(2,1)}, bf16[8,32,512]{2,1,0:T(8,128)(2,1)S(1)}, u32[]{:S(2)}) copy-start(bf16[8,32,512]{2,1,0:T(8,128)(2,1)S(1)} %all-to-all-done.6) | copy-start | bytes 786436
  66.6 76.9 %all-to-all-start.3 = ((bf16[8,768,512]{2,1,0:T(8,128)(2,1)}), bf16[8,768,512]{2,1,0:T(8,128)(2,1)}, u32[]{:S(2)}, u32[]{:S(2)}) async-start(bf16[8,768,512]{2,1,0:T(8,128)(2,1)} %broadcast_in_dim.99), calls=%async_computation.3 | async-start | bytes 12582912 | tf_op jit(solution)/shard_map/all_to_all | solution.py:17
  143.4 37.7 %all-to-all-start = ((bf16[8,2,128,512]{3,2,1,0:T(8,128)(2,1)}), bf16[8,2,128,512]{3,2,1,0:T(8,128)(2,1)}, u32[]{:S(2)}, u32[]{:S(2)}) async-start(bf16[8,2,128,512]{3,2,1,0:T(8,128)(2,1)} %bitcast_dynamic-update-slice_fusion), calls=%async_computation | async-start | bytes 4194304 | tf_op jit(solution)/shard_map/all_to_all | solution.py:128
  168.9 7.9 %copy-start.1 = (bf16[32,2,12,4096]{3,2,1,0:T(8,128)(2,1)S(1)}, bf16[32,2,12,4096]{3,2,1,0:T(8,128)(2,1)}, u32[]{:S(2)}) copy-start(bf16[32,2,12,4096]{3,2,1,0:T(8,128)(2,1)} %reshape_reshape.3) | copy-start | bytes 18874372
  168.9 7.9 %copy-start.5 = (bf16[2,4096,128]{2,1,0:T(8,128)(2,1)S(1)}, bf16[2,4096,128]{2,1,0:T(8,128)(2,1)}, u32[]{:S(2)}) copy-start(bf16[2,4096,128]{2,1,0:T(8,128)(2,1)} %param.17) | copy-start | bytes 6291460
  182.6 5.8 %copy-start.2 = (bf16[4096,128]{1,0:T(8,128)(2,1)S(1)}, bf16[4096,128]{1,0:T(8,128)(2,1)}, u32[]{:S(2)}) copy-start(bf16[4096,128]{1,0:T(8,128)(2,1)} %param.19) | copy-start | bytes 3145732
  182.6 26.5 %all-to-all-start.4 = ((bf16[8,32,2,12,128]{4,1,3,2,0:T(8,128)(2,1)}), bf16[8,32,2,12,128]{4,1,3,2,0:T(8,128)(2,1)}, u32[]{:S(2)}, u32[]{:S(2)}) async-start(bf16[8,32,2,12,128]{4,1,3,2,0:T(8,128)(2,1)} %broadcast_in_dim.100), calls=%async_computation.4 | async-start | bytes 3145728 | tf_op jit(solution)/shard_map/all_to_all | solution.py:17
  209.1 10.8 %all-to-all-start.7 = ((bf16[8,32,512]{2,1,0:T(8,128)(2,1)}), bf16[8,32,512]{2,1,0:T(8,128)(2,1)S(1)}, u32[]{:S(2)}, u32[]{:S(2)}) async-start(bf16[8,32,512]{2,1,0:T(8,128)(2,1)} %bitcast.108), calls=%async_computation.7 | async-start | bytes 524288 | tf_op jit(solution)/shard_map/all_to_all | solution.py:38
  215.5 10.2 %copy-start.4 = (f32[32,8]{0,1:T(8,128)S(1)}, f32[32,8]{0,1:T(8,128)}, u32[]{:S(2)}) copy-start(f32[32,8]{0,1:T(8,128)} %param.14) | copy-start | bytes 3076
  219.9 27.7 %all-to-all-start.5 = ((bf16[32,2,12,512]{3,1,2,0:T(2,128)(2,1)}), bf16[32,2,12,512]{3,1,2,0:T(2,128)(2,1)S(1)}, u32[]{:S(2)}, u32[]{:S(2)}) async-start(bf16[32,2,12,512]{3,1,2,0:T(2,128)(2,1)} %copy.102), calls=%async_computation.5 | async-start | bytes 1572864 | tf_op jit(solution)/shard_map/all_to_all | solution.py:140
